TPU v7x, 32 devices: a whole 2x2x4 slice. The times are simulated.
32 devices in a mesh: gr: 2 (over y), fs: 4 (over z), tp: 4 (over x, core).
Axes of the slice: x: 2, y: 2, z: 4, core: 2. Of those that a mesh axis runs over, the one named last changes fastest.
Arguments:
- tokens: bfloat16 [4096, 2048], P(('gr', 'tp'), 'fs'), may hold values from -6 to 6
- routes: int32 [4096, 2], P(('gr', 'tp')), may hold values from 0 to 7, all different within a row; in each aligned block of 512 rows (0 to 511, 512 to 1023, ...) at most 192 rows name the same one
- route_weight: float32 [4096, 2], P(('gr', 'tp')), may hold values from 0.25 to 1
- norm_gain: float32 [2048], P(('gr', 'fs')), may hold values from 0.1 to 1.9
- gate_master: float32 [8, 2048, 2816], P(None, ('gr', 'fs'), 'tp'), may hold values from -0.125 to 0.125
- up_master: float32 [8, 2048, 2816], P(None, ('gr', 'fs'), 'tp'), may hold values from -0.125 to 0.125
- down_master: float32 [8, 2048, 2816], P(None, ('gr', 'fs'), 'tp'), may hold values from -0.109375 to 0.109375
Outputs:
- mixed_output: bfloat16 [4096, 2048], P(('gr', 'tp'), 'fs')
- gate_serving: bfloat16 [8, 2048, 2816], P('tp', None, 'fs')
- up_serving: bfloat16 [8, 2048, 2816], P('tp', None, 'fs')
- down_serving: bfloat16 [8, 2048, 2816], P('tp', None, 'fs')
Inputs may be any that keep to these rules, and one draw needn't show every extreme that they name: `routes`: each row names two different experts. Within the rows of one block of 512 tokens (one index of gr+tp) no expert is named by more than 192 rows, and in some blocks one expert is named by exactly 192.
All inputs are finite; a program needn't handle non-finite values.
Results may differ from a plain program's by a relative error of at most 0.0082.
Values may be sent and summed in bfloat16 or wider, within the bound.
A program may use at most 128 MiB of HBM per device.

v0:
```python
import functools

import jax
import jax.numpy as jnp
from jax import lax
from jax.experimental import pallas as pl
from jax.experimental.pallas import tpu as pltpu
from jax.sharding import PartitionSpec as P

norm_eps = 1e-06
MESH = pl.DeviceIdType.MESH


def slot_table(routes, experts, capacity):
    flat_routes = routes.reshape(-1)
    onehot = (flat_routes[:, None] == jnp.arange(experts, dtype=jnp.int32)[None, :]).astype(
        jnp.int32
    )
    running = jnp.cumsum(onehot, axis=0)
    slot_index = jnp.sum(onehot * (running - 1), axis=1)
    return flat_routes * capacity + slot_index


def spread_kernel(sizes, count, flipped, *refs):
    gr, fs, tp, sub, local_experts, rows = sizes
    ins, outs, relays = refs[:count], refs[count : 2 * count], refs[2 * count : 3 * count]
    bounce, tp_send, tp_recv, fs_send, fs_recv, gr_send, gr_recv, load_sem, store_sem = refs[
        3 * count :
    ]
    g, f, t = lax.axis_index("gr"), lax.axis_index("fs"), lax.axis_index("tp")
    blocks = [(w, j) for j in range(local_experts) for w in range(count)]

    barrier = pltpu.get_barrier_semaphore()
    for axis, me, size in (("gr", g, gr), ("fs", f, fs), ("tp", t, tp)):
        for d in range(1, size):
            pl.semaphore_signal(
                barrier, inc=1, device_id={axis: lax.rem(me + d, size)}, device_id_type=MESH
            )
    pl.semaphore_wait(barrier, gr + fs + tp - 3)

    def out_rows(c, group, source):
        w, j = blocks[c]
        start = pl.multiple_of((group * fs + source) * rows, rows)
        if flipped:
            return outs[w].at[j, :, pl.ds(start, rows)]
        return outs[w].at[j, pl.ds(start, rows)]

    def own(c, target, s):
        w, j = blocks[c]
        return ins[w].at[s, target * local_experts + j]

    def relay(c, source, s):
        w, j = blocks[c]
        return relays[w].at[j, source, s]

    def tp_copy(c, d, s, to_out):
        target = lax.rem(t + d, tp)
        return pltpu.make_async_remote_copy(
            src_ref=own(c, target, s),
            dst_ref=out_rows(c, g, f) if to_out else relay(c, t, s),
            send_sem=tp_send.at[c, d, s],
            recv_sem=tp_recv.at[c, d, s],
            device_id={"tp": target},
            device_id_type=MESH,
        )

    def fs_copy(c, d, s, src, target):
        return pltpu.make_async_remote_copy(
            src_ref=src,
            dst_ref=out_rows(c, g, f),
            send_sem=fs_send.at[c, d, s],
            recv_sem=fs_recv.at[c, f],
            device_id={"fs": target},
            device_id_type=MESH,
        )

    def gr_copy(c, n, source, src):
        return pltpu.make_async_remote_copy(
            src_ref=src,
            dst_ref=out_rows(c, g, source),
            send_sem=gr_send.at[c, n, source],
            recv_sem=gr_recv.at[c, n, source],
            device_id={"gr": lax.rem(g + n, gr)},
            device_id_type=MESH,
        )

    def to_groups(c, source, src):
        for n in range(1, gr):
            gr_copy(c, n, source, src).start()

    def tp_start(c):
        for d in range(1, tp):
            for s in range(sub):

                @pl.when(t * sub + s == f)
                def _():
                    tp_copy(c, d, s, True).start()

                @pl.when(t * sub + s != f)
                def _():
                    tp_copy(c, d, s, False).start()

    def own_start(c):
        for s in range(sub):
            target = t * sub + s

            @pl.when(target != f)
            def _():
                fs_copy(c, 0, s, own(c, t, s), target).start()

            @pl.when(target == f)
            def _():
                pltpu.make_async_copy(own(c, t, s), bounce.at[c], load_sem.at[c]).start()
                to_groups(c, f, own(c, t, s))

    def own_store(c):
        for s in range(sub):

            @pl.when(t * sub + s == f)
            def _():
                pltpu.make_async_copy(own(c, t, s), bounce.at[c], load_sem.at[c]).wait()
                pltpu.make_async_copy(bounce.at[c], out_rows(c, g, f), store_sem.at[c]).start()

    def tp_arrived(c):
        for d in range(1, tp):
            source = lax.rem(t + tp - d, tp)
            for s in range(sub):
                target = source * sub + s

                @pl.when(target == f)
                def _():
                    tp_copy(c, d, s, True).wait_recv()
                    to_groups(c, f, out_rows(c, g, f))

                @pl.when(target != f)
                def _():
                    pltpu.make_async_remote_copy(
                        src_ref=own(c, t, s),
                        dst_ref=relay(c, source, s),
                        send_sem=tp_send.at[c, d, s],
                        recv_sem=tp_recv.at[c, d, s],
                        device_id={"tp": source},
                        device_id_type=MESH,
                    ).wait_recv()
                    fs_copy(c, d, s, relay(c, source, s), target).start()

    def fs_arrived(c):
        for d in range(1, fs):
            source = lax.rem(f + d, fs)
            pltpu.make_async_remote_copy(
                src_ref=own(c, t, 0),
                dst_ref=out_rows(c, g, source),
                send_sem=fs_send.at[c, 0, 0],
                recv_sem=fs_recv.at[c, source],
                device_id={"fs": source},
                device_id_type=MESH,
            ).wait_recv()
            to_groups(c, source, out_rows(c, g, source))

    total = len(blocks)
    ahead = min(3, total)
    own_start(0)
    for c in range(ahead):
        tp_start(c)
    for c in range(total + 1):
        if c + ahead < total:
            tp_start(c + ahead)
        if c + 1 < total:
            own_start(c + 1)
        if c < total:
            own_store(c)
            tp_arrived(c)
        if c >= 1:
            fs_arrived(c - 1)

    for c in range(total):
        for n in range(1, gr):
            for source in range(fs):
                group = lax.rem(g + gr - n, gr)
                pltpu.make_async_remote_copy(
                    src_ref=own(c, t, 0),
                    dst_ref=out_rows(c, group, source),
                    send_sem=gr_send.at[c, n, source],
                    recv_sem=gr_recv.at[c, n, source],
                    device_id={"gr": group},
                    device_id_type=MESH,
                ).wait_recv()
                gr_copy(c, n, source, out_rows(c, g, source)).wait_send()
        for s in range(sub):
            for d in range(1, tp):
                tp_copy(c, d, s, False).wait_send()
            for d in range(tp):
                target = lax.rem(t + tp - d, tp) * sub + s

                @pl.when(target != f)
                def _():
                    fs_copy(c, d, s, own(c, t, s), target).wait_send()

            @pl.when(t * sub + s == f)
            def _():
                pltpu.make_async_copy(bounce.at[c], out_rows(c, g, f), store_sem.at[c]).wait()


def spread(*weights):
    gr, fs, tp = lax.axis_size("gr"), lax.axis_size("fs"), lax.axis_size("tp")
    experts, rows, columns = weights[0].shape
    local_experts = experts // tp
    assert fs % tp == 0
    sub = fs // tp
    width = columns // sub
    count = len(weights)
    total = count * local_experts
    flipped = rows % 128 == 0
    order = (2, 0, 3, 1) if flipped else (2, 0, 1, 3)
    parts = [w.reshape(experts, rows, sub, width).transpose(order) for w in weights]
    block = (width, rows) if flipped else (rows, width)
    whole = (width, gr * fs * rows) if flipped else (gr * fs * rows, width)
    served = jax.ShapeDtypeStruct((local_experts, *whole), jnp.bfloat16)
    relayed = jax.ShapeDtypeStruct((local_experts, tp, sub, *block), jnp.bfloat16)
    dma = pltpu.SemaphoreType.DMA
    sent = 2 * total * rows * columns * (tp - 1 + fs - 1 + (gr - 1) * fs) // fs
    found = pl.pallas_call(
        functools.partial(spread_kernel, (gr, fs, tp, sub, local_experts, rows), count, flipped),
        out_shape=[served] * count + [relayed] * count,
        in_specs=[pl.BlockSpec(memory_space=pl.ANY)] * count,
        out_specs=[pl.BlockSpec(memory_space=pl.ANY)] * (2 * count),
        scratch_shapes=[
            pltpu.VMEM((total, *block), jnp.bfloat16),
            dma((total, tp, sub)),
            dma((total, tp, sub)),
            dma((total, tp, sub)),
            dma((total, fs)),
            dma((total, gr, fs)),
            dma((total, gr, fs)),
            dma((total,)),
            dma((total,)),
        ],
        compiler_params=pltpu.CompilerParams(collective_id=0, has_side_effects=True),
        cost_estimate=pl.CostEstimate(flops=0, bytes_accessed=40 * sent, transcendentals=0),
    )(*parts)
    return [w.swapaxes(1, 2) if flipped else w for w in found[:count]]


def local(tokens, routes, route_weight, norm_gain, gate_master, up_master, down_master):
    experts = gate_master.shape[0]
    tp_count = lax.axis_size("tp")
    fs_count = lax.axis_size("fs")
    local_experts = experts // tp_count
    token_rows = tokens.shape[0]
    model_width = tokens.shape[1] * fs_count
    capacity = 3 * token_rows // experts
    scaled_gain = norm_gain[None, :, None]
    gate_w = (gate_master * scaled_gain).astype(jnp.bfloat16)
    up_w = (up_master * scaled_gain).astype(jnp.bfloat16)
    down_w = down_master.astype(jnp.bfloat16)
    gate_w, up_w, down_w = spread(gate_w, up_w, down_w)
    as_float = tokens.astype(jnp.float32)
    square_total = lax.psum(jnp.sum(as_float * as_float, axis=1), "fs")
    normed = (as_float * lax.rsqrt(square_total / model_width + norm_eps)[:, None]).astype(
        jnp.bfloat16
    )
    placing = slot_table(routes, experts, capacity)
    slot_rows = jnp.arange(experts * capacity, dtype=jnp.int32)
    picked = (slot_rows[:, None] == placing[None, :]).reshape(experts * capacity, token_rows, 2)
    route_table = jnp.sum(picked.astype(jnp.float32), axis=2).astype(jnp.bfloat16)
    outgoing = jnp.dot(route_table, normed, preferred_element_type=jnp.float32).astype(jnp.bfloat16)
    outgoing = outgoing.reshape(tp_count, local_experts, capacity, tokens.shape[1])
    shard_piece = lax.all_gather(
        lax.all_to_all(outgoing, "tp", split_axis=0, concat_axis=0, tiled=True),
        "fs",
        axis=3,
        tiled=True,
    )
    returned = []
    for j in range(local_experts):
        rows = shard_piece[:, j]
        gate_acc = jnp.einsum("scd,df->scf", rows, gate_w[j], preferred_element_type=jnp.float32)
        up_acc = jnp.einsum("scd,df->scf", rows, up_w[j], preferred_element_type=jnp.float32)
        hidden = (jax.nn.silu(gate_acc) * up_acc).astype(jnp.bfloat16)
        partial_value = jnp.einsum(
            "scf,df->scd", hidden, down_w[j], preferred_element_type=jnp.float32
        )
        summed = lax.psum_scatter(
            partial_value.astype(jnp.bfloat16), "fs", scatter_dimension=2, tiled=True
        )
        returned.append(lax.all_to_all(summed, "tp", split_axis=0, concat_axis=0, tiled=True))
    produced = jnp.stack(returned, axis=1)
    produced = produced.reshape(experts * capacity, produced.shape[3])
    pair_slots = placing.reshape(token_rows, 2)
    first_rows = jnp.take(produced, pair_slots[:, 0], axis=0)
    second_rows = jnp.take(produced, pair_slots[:, 1], axis=0)
    mixed_out = first_rows * route_weight[:, 0:1] + second_rows * route_weight[:, 1:2]
    return (mixed_out.astype(jnp.bfloat16), gate_w, up_w, down_w)


def solution(mesh):
    placed = (
        P(("gr", "tp"), "fs"),
        P(("gr", "tp"), None),
        P(("gr", "tp"), None),
        P(("gr", "fs")),
        P(None, ("gr", "fs"), "tp"),
        P(None, ("gr", "fs"), "tp"),
        P(None, ("gr", "fs"), "tp"),
    )
    return jax.shard_map(
        local,
        mesh=mesh,
        in_specs=placed,
        out_specs=(
            P(("gr", "tp"), "fs"),
            P("tp", None, "fs"),
            P("tp", None, "fs"),
            P("tp", None, "fs"),
        ),
        check_vma=False,
    )
```

profile of v0, /device:TPU:0, one launch (start us, length us, event | category | flops | bytes accessed | tf_op | source)
XLA Modules:
  0.0 573.9 jit_solution(8462584864646491723)
XLA Ops:
  8.5 2.3 reduce-window.6
  12.3 1.5 convert_reduce_fusion
  14.0 13.5 %psum.7 = f32[512]{0:T(512)S(1)} all-reduce(f32[512]{0:T(512)S(1)} %fusion.9), channel_id=1, replica_groups=mesh['gr'=2,'fs'=4,'tp'=4] {'fs'}, use_global_device_ids=true, to_apply=%region_5.6 | all-reduce | flops 512 | bytes 4096 | tf_op jit(solution)/shard_map/psum | solution.py:258
  27.5 1.1 convolution_convert_fusion.2
  28.6 22.6 %all_to_all.15 = bf16[4,2,192,512]{3,2,1,0:T(8,128)(2,1)S(1)} all-to-all(bf16[4,2,192,512]{3,2,1,0:T(8,128)(2,1)S(1)} %bitcast.104), channel_id=1, replica_groups=mesh['gr'=2,'fs'=4,'tp'=4] {'tp'}, dimensions={0} | all-to-all | bytes 3145728 | tf_op jit(solution)/shard_map/all_to_all | solution.py:269
  51.2 1.3 copy.41
  52.7 4.5 convert_bitcast_fusion.refs_2_
  57.3 9.1 %fusion.1 = (bf16[1,8,704,256]{3,2,1,0:T(8,128)(2,1)}, bf16[1,8,704,256]{3,2,1,0:T(8,128)(2,1)}) fusion(f32[8,256,704]{1,2,0:T(8,128)} %param.14, f32[256]{0:T(256)S(1)} %copy-done.2, f32[8,256,704]{1,2,0:T(8,128)} %param.13), kind=kLoop, calls=%fused_computation.12 | loop fusion | flops 5767168 | bytes 17302528 | tf_op jit(solution)/shard_map/transpose | solution.py:215
  66.3 297.0 %shard_map.102 = (bf16[2,704,2048]{2,1,0:T(8,128)(2,1)}, bf16[2,704,2048]{2,1,0:T(8,128)(2,1)}, bf16[2,704,2048]{2,1,0:T(8,128)(2,1)}, bf16[2,4,1,704,256]{4,3,2...) custom-call(bf16[1,8,704,256]{3,2,1,0:T(8,128)(2,1)} %get-tuple-element.16.refs_0_, ...), custom_call_target="tpu_custom_call" | custom-call | bytes 216268800 | tf_op jit(solution)/shard_map/pallas_call | solution.py:222
  363.4 6.8 %fusion.3 = f32[4,192,704]{2,1,0:T(8,128)} fusion(bf16[2,2048,704]{1,2,0:T(8,128)(2,1)} %bitcast.99, bf16[4,2,192,2048]{3,2,0,1:T(8,128)(2,1)} %all-gather.2.cloned.1.call-done), kind=kOutput, calls=%fused_computation.17 | convolution fusion | flops 2214592512 | bytes 8192000 | tf_op jit(solution)/shard_map/scd,df->scf/dot_general | solution.py:277
  370.2 11.8 %convolution_convert_fusion = bf16[4,192,2048]{2,1,0:T(8,128)(2,1)} fusion(bf16[2,2048,704]{1,2,0:T(8,128)(2,1)} %bitcast.89, f32[4,192,704]{2,1,0:T(8,128)} %fusion.3, bf16[2,2048,704]{1,2,0:T(8,128)(2,1)} %bitcast.94, bf16[4,2,192,2048]{3,2,0,1:T(8,128)(2,1)} %all-gather.2.cloned.1.call-done), kind=kOutput, calls=%fused_computation.6 | convolution fusion | flops 4434001920 | bytes 14417920 | tf_op jit(solution)/shard_map/scf,df->scd/dot_general | solution.py:280
  382.3 6.8 %fusion.5 = f32[4,192,704]{2,1,0:T(8,128)} fusion(bf16[2,2048,704]{1,2,0:T(8,128)(2,1)} %bitcast.100, bf16[4,2,192,2048]{3,2,0,1:T(8,128)(2,1)} %all-gather.2.cloned.1.call-done), kind=kOutput, calls=%fused_computation.22 | convolution fusion | flops 2214592512 | bytes 8192000 | tf_op jit(solution)/shard_map/scd,df->scf/dot_general | solution.py:277
  389.1 11.8 %convolution_convert_fusion.1 = bf16[4,192,2048]{2,1,0:T(8,128)(2,1)} fusion(bf16[2,2048,704]{1,2,0:T(8,128)(2,1)} %bitcast.90, f32[4,192,704]{2,1,0:T(8,128)} %fusion.5, bf16[2,2048,704]{1,2,0:T(8,128)(2,1)} %bitcast.95, bf16[4,2,192,2048]{3,2,0,1:T(8,128)(2,1)} %all-gather.2.cloned.1.call-done), kind=kOutput, calls=%fused_computation.7 | convolution fusion | flops 4434001920 | bytes 14417920 | tf_op jit(solution)/shard_map/scf,df->scd/dot_general | solution.py:280
  400.9 68.8 %reduce-scatter.5.cloned.1.call-done = bf16[4,192,512]{2,1,0:T(8,128)(2,1)} async-done(((bf16[4,192,2048]{2,1,0:T(8,128)(2,1)}), bf16[4,192,512]{2,1,0:T(8,128)(2,1)}) %reduce-scatter.5.cloned.1.call-update) | async-done | bytes 786448 | tf_op jit(solution)/shard_map/reduce_scatter | solution.py:283
  469.7 3.5 all-to-all-start.2
  473.2 59.7 %reduce-scatter.3.cloned.1.call-done = bf16[4,192,512]{2,1,0:T(8,128)(2,1)} async-done(((bf16[4,192,2048]{2,1,0:T(8,128)(2,1)}), bf16[4,192,512]{2,1,0:T(8,128)(2,1)}) %reduce-scatter.3.cloned.1.call-update) | async-done | bytes 786448 | tf_op jit(solution)/shard_map/reduce_scatter | solution.py:283
  532.9 3.5 all-to-all-start.1
  536.5 11.5 %all-to-all-done.1 = bf16[4,192,512]{2,1,0:T(8,128)(2,1)S(1)} async-done(((bf16[4,192,512]{2,1,0:T(8,128)(2,1)}), bf16[4,192,512]{2,1,0:T(8,128)(2,1)S(1)}, u32[]{:S(2)}, u32[]{:S(2)}) %all-to-all-start.1) | async-done | bytes 786464 | tf_op jit(solution)/shard_map/all_to_all | solution.py:286
  548.3 2.6 gather_fusion.1
  550.9 2.6 gather_fusion
  553.5 2.5 add_convert_fusion
  556.0 6.3 %copy.48 = bf16[2,2048,704]{1,2,0:T(8,128)(2,1)} copy(bf16[2,2048,704]{1,2,0:T(8,128)(2,1)} %bitcast.101) | data formatting | bytes 11534336
  562.3 2.5 copy.49
  564.9 2.5 copy.50
  (46 shorter events, 3.9 us)
Async XLA Ops:
  7.2 6.7 %copy-start = (bf16[512,512]{1,0:T(8,128)(2,1)S(1)}, bf16[512,512]{1,0:T(8,128)(2,1)}, u32[]{:S(2)}) copy-start(bf16[512,512]{1,0:T(8,128)(2,1)} %param.9) | copy-start | bytes 1572868
  7.2 356.2 %all-gather.2.cloned.1.call-start = ((), (), s32[]{:S(2)}) async-start(), calls=%async_computation.5 | async-start | bytes 7864320 | tf_op jit(solution)/shard_map/all_gather | solution.py:268
  52.5 4.8 copy-start.2
  52.5 417.2 %reduce-scatter.5.cloned.1.call-start = ((), (), s32[]{:S(2)}) async-start(), calls=%async_computation.7 | async-start | bytes 3932160 | tf_op jit(solution)/shard_map/reduce_scatter | solution.py:283
  382.0 150.9 %reduce-scatter.3.cloned.1.call-start = ((), (), s32[]{:S(2)}) async-start(), calls=%async_computation.6 | async-start | bytes 3932160 | tf_op jit(solution)/shard_map/reduce_scatter | solution.py:283
  400.9 135.6 %copy-start.1 = (f32[512,2]{0,1:T(2,128)S(1)}, f32[512,2]{0,1:T(2,128)}, u32[]{:S(2)}) copy-start(f32[512,2]{0,1:T(2,128)} %param.11) | copy-start | bytes 12292
  469.7 63.2 %all-to-all-start.2 = ((bf16[4,192,512]{2,1,0:T(8,128)(2,1)}), bf16[4,192,512]{2,1,0:T(8,128)(2,1)S(1)}, u32[]{:S(2)}, u32[]{:S(2)}) async-start(bf16[4,192,512]{2,1,0:T(8,128)(2,1)} %reduce-scatter.5.cloned.1.call-done), calls=%async_computation.4 | async-start | bytes 1572864 | tf_op jit(solution)/shard_map/all_to_all | solution.py:286
  532.9 15.1 %all-to-all-start.1 = ((bf16[4,192,512]{2,1,0:T(8,128)(2,1)}), bf16[4,192,512]{2,1,0:T(8,128)(2,1)S(1)}, u32[]{:S(2)}, u32[]{:S(2)}) async-start(bf16[4,192,512]{2,1,0:T(8,128)(2,1)} %reduce-scatter.3.cloned.1.call-done), calls=%async_computation.2 | async-start | bytes 1572864 | tf_op jit(solution)/shard_map/all_to_all | solution.py:286
  548.2 14.2 %slice-start.2 = ((s8[5767168]{0:T(1024)(128)(4,1)}), s8[1572864]{0:T(1024)(128)(4,1)S(1)}, s32[]{:S(2)}) async-start(s8[5767168]{0:T(1024)(128)(4,1)} %bitcast.96), calls=%async_computation.10 | async-start | bytes 3145728
  553.5 8.8 %slice-start.3 = ((s8[5767168]{0:T(1024)(128)(4,1)}), s8[4194304]{0:T(1024)(128)(4,1)S(1)}, s32[]{:S(2)}) async-start(s8[5767168]{0:T(1024)(128)(4,1)} %bitcast.96), calls=%async_computation.11 | async-start | bytes 8388608
  556.0 8.9 %slice-start = ((s8[5767168]{0:T(1024)(128)(4,1)}), s8[4194304]{0:T(1024)(128)(4,1)S(1)}, s32[]{:S(2)}) async-start(s8[5767168]{0:T(1024)(128)(4,1)} %bitcast.91), calls=%async_computation.8 | async-start | bytes 8388608
  562.3 2.5 slice-start.1
Sparse Core Ops, SparseCore 0:
  52.6 252.8 all-gather.1
  382.1 87.5 reduce-scatter.4
  472.6 60.3 reduce-scatter.2
where the time goes:
time: 574 us
  Pallas kernels  297 us (52%)
  waiting for transfers between devices  140 us (24%)
  matrix products  38.2 us (7%)
  blocking collectives  36.1 us (6%)
  other arithmetic  21.2 us (4%)
  local copies, waits for them, and re-layouts  19.8 us (3%)
  between operations  13.9 us (2%)
  starting transfers between devices  7.51 us (1%)
    pallas_call x1, Pallas kernels, spread(): pl.pallas_call(functools.partial(spread_kernel, (gr, fs, tp, sub, local_e...  297 us
    reduce_scatter x2, waiting for transfers between devices, local(): lax.psum_scatter(partial_value.astype(jnp.bfloat16), 'fs', scatter_dimens...  128 us
    dot_general x2, matrix products, local(): jnp.einsum('scf,df->scd', hidden, down_w[j], preferred_element_type=jnp.f...  23.5 us
    all_to_all x1, blocking collectives, local(): lax.all_to_all(outgoing, 'tp', split_axis=0, concat_axis=0, tiled=True)  22.6 us
    dot_general x2, matrix products, local(): jnp.einsum('scd,df->scf', rows, gate_w[j], preferred_element_type=jnp.flo...  13.6 us
    transpose x2, other arithmetic, spread(): w.reshape(experts, rows, sub, width).transpose(order)  13.6 us
    psum x1, blocking collectives, local(): square_total = lax.psum(jnp.sum(as_float * as_float, axis=1), 'fs')  13.5 us
    unnamed x18, local copies, waits for them, and re-layouts  12.3 us
  transfers between devices with their start and end apart: 5, of which 3 were waited for; matrix products, arithmetic and copies ran while one was open for 6% of the time, Pallas kernels for 52%

commit v1 on v0

--- a/solution.py
+++ b/solution.py
@@ -241,7 +241,7 @@
     return [w.swapaxes(1, 2) if flipped else w for w in found[:count]]
 
 
-def local(tokens, routes, route_weight, norm_gain, gate_master, up_master, down_master):
+def local_by_collectives(tokens, routes, route_weight, norm_gain, gate_master, up_master, down_master):
     experts = gate_master.shape[0]
     tp_count = lax.axis_size("tp")
     fs_count = lax.axis_size("fs")
@@ -293,6 +293,554 @@
     return (mixed_out.astype(jnp.bfloat16), gate_w, up_w, down_w)
 
 
+def slot_places(routes, experts, capacity):
+    rows = routes.shape[0]
+    hits = (routes[:, :, None] == jnp.arange(experts, dtype=jnp.int32)).astype(jnp.int32)
+    both = hits[:, 0] + hits[:, 1]
+    before = jnp.cumsum(both, axis=0) - both
+    first = jnp.sum(hits[:, 0] * before, axis=1)
+    second = jnp.sum(hits[:, 1] * (before + hits[:, 0]), axis=1)
+    places = jnp.stack([first, second]) + routes.T * capacity
+    return jnp.pad(places, ((0, 6), (0, 0)))
+
+
+def serve_kernel(sizes, *refs):
+    gr, fs, tp, local_experts, rows, capacity = sizes
+    tokens, places, shares = refs[:3]
+    ins, outs, relays, partial = refs[3:6], refs[6:9], refs[9:12], refs[12]
+    (
+        bounce, gathered, place_of, share_of, picks, slot_share, slots, hid, spread_hid,
+        gate_buf, up_buf, down_buf, part_buf,
+        tp_send, tp_recv, fs_send, fs_recv, gr_send, gr_recv, load_sem, store_sem,
+        tokz_send, tokz_recv, tokt_send, tokt_recv, info_send, info_recv, own_sem,
+        weight_sem, down_sem, part_sem,
+    ) = refs[13:]
+    count = 3
+    g, f, t = lax.axis_index("gr"), lax.axis_index("fs"), lax.axis_index("tp")
+    blocks = [(w, j) for j in range(local_experts) for w in range(2)]
+    blocks += [(2, j) for j in range(local_experts)]
+    total = len(blocks)
+    token_rows, features = tokens.shape
+    width = gathered.shape[2]
+
+    barrier = pltpu.get_barrier_semaphore()
+    for axis, me, size in (("gr", g, gr), ("fs", f, fs), ("tp", t, tp)):
+        for d in range(1, size):
+            pl.semaphore_signal(
+                barrier, inc=1, device_id={axis: lax.rem(me + d, size)}, device_id_type=MESH
+            )
+    pl.semaphore_wait(barrier, gr + fs + tp - 3)
+
+    def remote(src, dst, send, recv, axis, target):
+        return pltpu.make_async_remote_copy(
+            src_ref=src, dst_ref=dst, send_sem=send, recv_sem=recv,
+            device_id={axis: target}, device_id_type=MESH,
+        )
+
+    def slab(block, source):
+        start = pl.multiple_of(source * features, features)
+        return gathered.at[block, :, pl.ds(start, features)]
+
+    def tokz(d):
+        return remote(
+            tokens, slab(t, f), tokz_send.at[d], tokz_recv.at[f], "fs", lax.rem(f + d, fs)
+        )
+
+    def tokz_from(d):
+        source = lax.rem(f + fs - d, fs)
+        return source, remote(
+            tokens, slab(t, source), tokz_send.at[d], tokz_recv.at[source], "fs", source
+        )
+
+    def tokt(d, source):
+        return remote(
+            slab(t, source), slab(t, source), tokt_send.at[d, source], tokt_recv.at[t, source],
+            "tp", lax.rem(t + d, tp),
+        )
+
+    def info(d, k):
+        whole = (place_of, share_of)[k]
+        return remote(
+            (places, shares)[k], whole.at[t], info_send.at[d, k], info_recv.at[t, k],
+            "tp", lax.rem(t + d, tp),
+        )
+
+    def own_copies():
+        return (
+            pltpu.make_async_copy(tokens, slab(t, f), own_sem.at[0]),
+            pltpu.make_async_copy(places, place_of.at[t], own_sem.at[1]),
+            pltpu.make_async_copy(shares, share_of.at[t], own_sem.at[2]),
+        )
+
+    def out_rows(c, group, source):
+        w, j = blocks[c]
+        start = pl.multiple_of((group * fs + source) * rows, rows)
+        return outs[w].at[j, :, pl.ds(start, rows)]
+
+    def own(c, target):
+        w, j = blocks[c]
+        return ins[w].at[target * local_experts + j]
+
+    def relay(c, source):
+        w, j = blocks[c]
+        return relays[w].at[j, source]
+
+    def tp_copy(c, d, to_out):
+        target = lax.rem(t + d, tp)
+        return remote(
+            own(c, target), out_rows(c, g, f) if to_out else relay(c, t),
+            tp_send.at[c, d], tp_recv.at[c, d], "tp", target,
+        )
+
+    def fs_copy(c, d, src, target):
+        return remote(src, out_rows(c, g, f), fs_send.at[c, d], fs_recv.at[c, f], "fs", target)
+
+    def gr_copy(c, n, source, src):
+        return remote(
+            src, out_rows(c, g, source), gr_send.at[c, n, source], gr_recv.at[c, n, source],
+            "gr", lax.rem(g + n, gr),
+        )
+
+    def to_groups(c, source, src):
+        for n in range(1, gr):
+            gr_copy(c, n, source, src).start()
+
+    def tp_start(c):
+        for d in range(1, tp):
+
+            @pl.when(t == f)
+            def _():
+                tp_copy(c, d, True).start()
+
+            @pl.when(t != f)
+            def _():
+                tp_copy(c, d, False).start()
+
+    def own_start(c):
+        @pl.when(t != f)
+        def _():
+            fs_copy(c, 0, own(c, t), t).start()
+
+        @pl.when(t == f)
+        def _():
+            pltpu.make_async_copy(own(c, t), bounce.at[c], load_sem.at[c]).start()
+            to_groups(c, f, own(c, t))
+
+    def own_store(c):
+        @pl.when(t == f)
+        def _():
+            pltpu.make_async_copy(own(c, t), bounce.at[c], load_sem.at[c]).wait()
+            pltpu.make_async_copy(bounce.at[c], out_rows(c, g, f), store_sem.at[c]).start()
+
+    def tp_arrived(c):
+        for d in range(1, tp):
+            source = lax.rem(t + tp - d, tp)
+
+            @pl.when(source == f)
+            def _():
+                tp_copy(c, d, True).wait_recv()
+                to_groups(c, f, out_rows(c, g, f))
+
+            @pl.when(source != f)
+            def _():
+                remote(
+                    own(c, t), relay(c, source), tp_send.at[c, d], tp_recv.at[c, d], "tp", source
+                ).wait_recv()
+                fs_copy(c, d, relay(c, source), source).start()
+
+    def fs_arrived(c):
+        for d in range(1, fs):
+            source = lax.rem(f + d, fs)
+            remote(
+                own(c, t), out_rows(c, g, source), fs_send.at[c, 0], fs_recv.at[c, source],
+                "fs", source,
+            ).wait_recv()
+            to_groups(c, source, out_rows(c, g, source))
+
+    def gr_arrived(c):
+        for n in range(1, gr):
+            for source in range(fs):
+                group = lax.rem(g + gr - n, gr)
+                remote(
+                    own(c, t), out_rows(c, group, source), gr_send.at[c, n, source],
+                    gr_recv.at[c, n, source], "gr", group,
+                ).wait_recv()
+
+    def own_stored(c):
+        @pl.when(t == f)
+        def _():
+            pltpu.make_async_copy(bounce.at[c], out_rows(c, g, f), store_sem.at[c]).wait()
+
+    def sent(c):
+        for n in range(1, gr):
+            for source in range(fs):
+                gr_copy(c, n, source, out_rows(c, g, source)).wait_send()
+        for d in range(1, tp):
+            tp_copy(c, d, False).wait_send()
+        for d in range(tp):
+            target = lax.rem(t + tp - d, tp)
+
+            @pl.when(target != f)
+            def _():
+                fs_copy(c, d, own(c, t), target).wait_send()
+
+    def pick_slots(j):
+        @pl.loop(0, tp)
+        def _(b):
+            base = (t * local_experts + j) * capacity
+            index = lax.broadcasted_iota(jnp.int32, (capacity, token_rows), 0) + base
+            first = place_of[b, 0:1, :] == index
+            second = place_of[b, 1:2, :] == index
+            share = jnp.where(first, share_of[b, 0:1, :], 0.0)
+            share = share + jnp.where(second, share_of[b, 1:2, :], 0.0)
+            share = jnp.sum(share, axis=1, keepdims=True)
+            at = pl.ds(pl.multiple_of(b * capacity, capacity), capacity)
+            slot_share[at, :] = jnp.broadcast_to(share, (capacity, 128))
+            pick = jnp.where(first | second, 1.0, 0.0).astype(jnp.bfloat16)
+            picks[b] = pick
+            squares = jnp.zeros((capacity, 1), jnp.float32)
+            for q in range(fs):
+                columns = slice(q * features, (q + 1) * features)
+                raw = jnp.dot(
+                    pick, gathered[b, :, columns], preferred_element_type=jnp.float32
+                )
+                slots[at, columns] = raw.astype(jnp.bfloat16)
+                squares = squares + jnp.sum(raw * raw, axis=1, keepdims=True)
+            scale = lax.rsqrt(squares / width + norm_eps)
+            for q in range(fs):
+                columns = slice(q * features, (q + 1) * features)
+                raw = slots[at, columns].astype(jnp.float32)
+                slots[at, columns] = (raw * scale).astype(jnp.bfloat16)
+
+    def weight_load(w, j):
+        return pltpu.make_async_copy(outs[w].at[j], (gate_buf, up_buf)[w], weight_sem.at[w])
+
+    def hidden_of(j):
+        units = gate_buf.shape[0]
+        step = 2 * capacity
+        for start in range(0, units, 256):
+            cut = slice(start, min(start + 256, units))
+
+            @pl.loop(0, tp * capacity // step)
+            def _(m):
+                at = pl.ds(pl.multiple_of(m * step, step), step)
+                into = (((1,), (1,)), ((), ()))
+                gate = lax.dot_general(
+                    slots[at, :], gate_buf[cut, :], into, preferred_element_type=jnp.float32
+                )
+                up = lax.dot_general(
+                    slots[at, :], up_buf[cut, :], into, preferred_element_type=jnp.float32
+                )
+                value = gate / (1.0 + jnp.exp(-gate)) * up
+                hid[at, cut] = (value * slot_share[at, 0:1]).astype(jnp.bfloat16)
+
+    def hidden_to_tokens(j):
+        @pl.loop(0, tp)
+        def _(b):
+            at = pl.ds(pl.multiple_of(b * capacity, capacity), capacity)
+            spread_hid[j, b] = lax.dot_general(
+                picks[b], hid[at, :], (((0,), (0,)), ((), ())),
+                preferred_element_type=jnp.float32,
+            ).astype(jnp.bfloat16)
+
+    def down_load(r, j):
+        start = pl.multiple_of(r * rows, rows)
+        return pltpu.make_async_copy(
+            outs[2].at[j, :, pl.ds(start, rows)], down_buf.at[r % 2, j], down_sem.at[r % 2, j]
+        )
+
+    def part_store(r, b):
+        start = pl.multiple_of(r * rows, rows)
+        return pltpu.make_async_copy(
+            part_buf.at[r % 2, b], partial.at[b, :, pl.ds(start, rows)], part_sem.at[r % 2, b]
+        )
+
+    def part_of(r):
+        @pl.loop(0, tp)
+        def _(b):
+            value = jnp.dot(
+                spread_hid[0, b], down_buf[r % 2, 0], preferred_element_type=jnp.float32
+            )
+            for j in range(1, local_experts):
+                value = value + jnp.dot(
+                    spread_hid[j, b], down_buf[r % 2, j], preferred_element_type=jnp.float32
+                )
+            part_buf[r % 2, b] = value.astype(jnp.bfloat16)
+            part_store(r, b).start()
+
+    for d in range(1, fs):
+        tokz(d).start()
+    for copy in own_copies():
+        copy.start()
+    own_start(0)
+    for d in range(1, tp):
+        for k in range(2):
+            info(d, k).start()
+    tp_start(0)
+    for copy in own_copies():
+        copy.wait()
+    for d in range(1, tp):
+        tokt(d, f).start()
+    ahead = min(3, total)
+    for c in range(1, ahead):
+        tp_start(c)
+    for d in range(1, fs):
+        source, copy = tokz_from(d)
+        copy.wait_recv()
+        for e in range(1, tp):
+            tokt(e, source).start()
+
+    for c in range(total + 1):
+        if c + ahead < total:
+            tp_start(c + ahead)
+        if c + 1 < total:
+            own_start(c + 1)
+        if c < total:
+            own_store(c)
+            tp_arrived(c)
+        if c >= 1:
+            fs_arrived(c - 1)
+    for c in range(total):
+        gr_arrived(c)
+        own_stored(c)
+
+    for d in range(1, tp):
+        source = lax.rem(t + d, tp)
+        for k in range(2):
+            whole = (place_of, share_of)[k]
+            remote(
+                (places, shares)[k], whole.at[source], info_send.at[d, k],
+                info_recv.at[source, k], "tp", source,
+            ).wait_recv()
+        for s in range(fs):
+            remote(
+                slab(source, s), slab(source, s), tokt_send.at[d, s], tokt_recv.at[source, s],
+                "tp", source,
+            ).wait_recv()
+    for j in range(local_experts):
+        weight_load(0, j).start()
+        weight_load(1, j).start()
+        pick_slots(j)
+        weight_load(0, j).wait()
+        weight_load(1, j).wait()
+        hidden_of(j)
+        hidden_to_tokens(j)
+    blocks_down = gr * fs
+    for r in range(blocks_down):
+        for j in range(local_experts):
+            if r == 0:
+                down_load(r, j).start()
+            if r + 1 < blocks_down:
+                down_load(r + 1, j).start()
+        for j in range(local_experts):
+            down_load(r, j).wait()
+        if r >= 2:
+            for b in range(tp):
+                part_store(r - 2, b).wait()
+        part_of(r)
+    for r in range(max(0, blocks_down - 2), blocks_down):
+        for b in range(tp):
+            part_store(r, b).wait()
+
+    for c in range(total):
+        sent(c)
+    for d in range(1, fs):
+        tokz(d).wait_send()
+    for d in range(1, tp):
+        for s in range(fs):
+            tokt(d, s).wait_send()
+        for k in range(2):
+            info(d, k).wait_send()
+
+
+def serve(tokens, places, shares, capacity, *weights):
+    gr, fs, tp = lax.axis_size("gr"), lax.axis_size("fs"), lax.axis_size("tp")
+    experts, rows, columns = weights[0].shape
+    local_experts = experts // tp
+    token_rows, features = tokens.shape
+    width = features * fs
+    parts = [w.transpose(0, 2, 1) for w in weights]
+    total = 3 * local_experts
+    block = (columns, rows)
+    bf16, f32 = jnp.bfloat16, jnp.float32
+    served = jax.ShapeDtypeStruct((local_experts, columns, width), bf16)
+    relayed = jax.ShapeDtypeStruct((local_experts, tp, *block), bf16)
+    dma = pltpu.SemaphoreType.DMA
+    anywhere = pl.BlockSpec(memory_space=pl.ANY)
+    slots = tp * capacity
+    found = pl.pallas_call(
+        functools.partial(serve_kernel, (gr, fs, tp, local_experts, rows, capacity)),
+        out_shape=[served] * 3
+        + [relayed] * 3
+        + [jax.ShapeDtypeStruct((tp, token_rows, width), bf16)],
+        in_specs=[anywhere] * 6,
+        out_specs=[anywhere] * 7,
+        scratch_shapes=[
+            pltpu.VMEM((total, *block), bf16),
+            pltpu.VMEM((tp, token_rows, width), bf16),
+            pltpu.VMEM((tp, *places.shape), jnp.int32),
+            pltpu.VMEM((tp, *shares.shape), f32),
+            pltpu.VMEM((tp, capacity, token_rows), bf16),
+            pltpu.VMEM((slots, 128), f32),
+            pltpu.VMEM((slots, width), bf16),
+            pltpu.VMEM((slots, columns), bf16),
+            pltpu.VMEM((local_experts, tp, token_rows, columns), bf16),
+            pltpu.VMEM((columns, width), bf16),
+            pltpu.VMEM((columns, width), bf16),
+            pltpu.VMEM((2, local_experts, columns, rows), bf16),
+            pltpu.VMEM((2, tp, token_rows, rows), bf16),
+            dma((total, tp)),
+            dma((total, tp)),
+            dma((total, tp)),
+            dma((total, fs)),
+            dma((total, gr, fs)),
+            dma((total, gr, fs)),
+            dma((total,)),
+            dma((total,)),
+            dma((fs,)),
+            dma((fs,)),
+            dma((tp, fs)),
+            dma((tp, fs)),
+            dma((tp, 2)),
+            dma((tp, 2)),
+            dma((3,)),
+            dma((2,)),
+            dma((2, local_experts)),
+            dma((2, tp)),
+        ],
+        compiler_params=pltpu.CompilerParams(
+            collective_id=0, has_side_effects=True, vmem_limit_bytes=60 * 1024 * 1024
+        ),
+        name="serve",
+    )(tokens, places, shares, *parts)
+    return [w.swapaxes(1, 2) for w in found[:3]], found[6]
+
+
+def combine_kernel(sizes, *refs):
+    fs, tp = sizes
+    partial, out = refs[:2]
+    (
+        mine, arrived, shared, reduced, total,
+        load_sem, tp_send, tp_recv, fs_send, fs_recv, store_sem,
+    ) = refs[2:]
+    f, t = lax.axis_index("fs"), lax.axis_index("tp")
+    features = out.shape[1]
+
+    barrier = pltpu.get_barrier_semaphore()
+    for axis, me, size in (("fs", f, fs), ("tp", t, tp)):
+        for d in range(1, size):
+            pl.semaphore_signal(
+                barrier, inc=1, device_id={axis: lax.rem(me + d, size)}, device_id_type=MESH
+            )
+    pl.semaphore_wait(barrier, fs + tp - 2)
+
+    def cut(block, q):
+        start = pl.multiple_of(q * features, features)
+        return partial.at[block, :, pl.ds(start, features)]
+
+    def tp_copy(e, d):
+        q = lax.rem(f + e, fs)
+        target = lax.rem(t + d, tp)
+        return pltpu.make_async_remote_copy(
+            src_ref=cut(target, q), dst_ref=arrived.at[e % fs, d], send_sem=tp_send.at[e % fs, d],
+            recv_sem=tp_recv.at[e % fs, d], device_id={"tp": target}, device_id_type=MESH,
+        )
+
+    def load(e):
+        return pltpu.make_async_copy(
+            cut(t, lax.rem(f + e, fs)), mine.at[e % fs], load_sem.at[e % fs]
+        )
+
+    def fs_copy(e):
+        return pltpu.make_async_remote_copy(
+            src_ref=shared.at[e], dst_ref=reduced.at[e], send_sem=fs_send.at[e],
+            recv_sem=fs_recv.at[e], device_id={"fs": lax.rem(f + e, fs)}, device_id_type=MESH,
+        )
+
+    order = list(range(1, fs)) + [fs]
+    for e in order:
+        load(e).start()
+        for d in range(1, tp):
+            tp_copy(e, d).start()
+    for e in order:
+        load(e).wait()
+        for d in range(1, tp):
+            tp_copy(e, d).wait_recv()
+        value = mine[e % fs].astype(jnp.float32)
+        for d in range(1, tp):
+            value = value + arrived[e % fs, d].astype(jnp.float32)
+        if e < fs:
+            shared[e] = value.astype(jnp.bfloat16)
+            fs_copy(e).start()
+        else:
+            total[...] = value
+    value = total[...]
+    for e in range(1, fs):
+        fs_copy(e).wait_recv()
+        value = value + reduced[e].astype(jnp.float32)
+    mine[0] = value.astype(jnp.bfloat16)
+    store = pltpu.make_async_copy(mine.at[0], out, store_sem)
+    store.start()
+    for e in order:
+        for d in range(1, tp):
+            tp_copy(e, d).wait_send()
+        if e < fs:
+            fs_copy(e).wait_send()
+    store.wait()
+
+
+def combine(partial):
+    fs, tp = lax.axis_size("fs"), lax.axis_size("tp")
+    _, token_rows, width = partial.shape
+    features = width // fs
+    block = (token_rows, features)
+    bf16 = jnp.bfloat16
+    dma = pltpu.SemaphoreType.DMA
+    return pl.pallas_call(
+        functools.partial(combine_kernel, (fs, tp)),
+        out_shape=jax.ShapeDtypeStruct(block, bf16),
+        in_specs=[pl.BlockSpec(memory_space=pl.ANY)],
+        out_specs=pl.BlockSpec(memory_space=pl.ANY),
+        scratch_shapes=[
+            pltpu.VMEM((fs, *block), bf16),
+            pltpu.VMEM((fs, tp, *block), bf16),
+            pltpu.VMEM((fs, *block), bf16),
+            pltpu.VMEM((fs, *block), bf16),
+            pltpu.VMEM(block, jnp.float32),
+            dma((fs,)),
+            dma((fs, tp)),
+            dma((fs, tp)),
+            dma((fs,)),
+            dma((fs,)),
+            dma,
+        ],
+        compiler_params=pltpu.CompilerParams(
+            collective_id=1, has_side_effects=True, vmem_limit_bytes=48 * 1024 * 1024
+        ),
+        name="combine",
+    )(partial)
+
+
+def local(tokens, routes, route_weight, norm_gain, gate_master, up_master, down_master):
+    experts, rows, columns = gate_master.shape
+    gr, fs, tp = lax.axis_size("gr"), lax.axis_size("fs"), lax.axis_size("tp")
+    token_rows, features = tokens.shape
+    capacity = 3 * token_rows // experts
+    fits = fs == tp and rows % 128 == 0 and features % 128 == 0 and features % rows == 0
+    if not (fits and gr == 2 and capacity % 16 == 0 and columns % 16 == 0):
+        return local_by_collectives(
+            tokens, routes, route_weight, norm_gain, gate_master, up_master, down_master
+        )
+    scaled_gain = norm_gain[None, :, None]
+    gate_w = (gate_master * scaled_gain).astype(jnp.bfloat16)
+    up_w = (up_master * scaled_gain).astype(jnp.bfloat16)
+    down_w = down_master.astype(jnp.bfloat16)
+    places = slot_places(routes, experts, capacity)
+    shares = jnp.pad(route_weight.T, ((0, 6), (0, 0)))
+    served, partial = serve(tokens, places, shares, capacity, gate_w, up_w, down_w)
+    return (combine(partial), *served)
+
+
 def solution(mesh):
     placed = (
         P(("gr", "tp"), "fs"),

time: 574 us -> 445 us (0.78); the launches traced: 574 us -> 438 us
  waiting for transfers between devices: 140 us -> 0 us
  Pallas kernels: 297 us -> 410 us
  matrix products: 38.2 us -> 0 us
  blocking collectives: 36.1 us -> 0 us
  between operations: 13.9 us -> 0.69 us
  starting transfers between devices: 7.51 us -> 0 us
  other arithmetic: 21.2 us -> 13.9 us
  local copies, waits for them, and re-layouts: 19.8 us -> 13.3 us
    reduce_scatter x2 -> x0, waiting for transfers between devices: 128 us -> none  [local(): lax.psum_scatter(partial_value.astype(jnp.bfloat16), 'fs', scatter_dimens...]
    pallas_call x1 -> x2, Pallas kernels: 297 us -> 410 us  [the longest x1 298 us: serve(): pl.pallas_call(functools.partial(serve_kernel, (gr, fs, tp, local_experts...]
    dot_general x5 -> x0, matrix products: 38.2 us -> none  [the longest x2 23.5 us: local(): jnp.einsum('scf,df->scd', hidden, down_w[j], preferred_element_type=jnp.f...]
    all_to_all x1 -> x0, blocking collectives: 22.6 us -> none  [local(): lax.all_to_all(outgoing, 'tp', split_axis=0, concat_axis=0, tiled=True)]
    psum x1 -> x0, blocking collectives: 13.5 us -> none  [local(): square_total = lax.psum(jnp.sum(as_float * as_float, axis=1), 'fs')]
    all_to_all x2 -> x0, waiting for transfers between devices: 11.5 us -> none  [local(): lax.all_to_all(summed, 'tp', split_axis=0, concat_axis=0, tiled=True)]
    all_to_all x2 -> x0, starting transfers between devices: 6.99 us -> none  [local(): lax.all_to_all(summed, 'tp', split_axis=0, concat_axis=0, tiled=True)]
    unnamed x18 -> x16, local copies, waits for them, and re-layouts: 12.3 us -> 11.2 us
  transfers between devices with their start and end apart: 5 -> 0, of which waited for: 3 -> 0; matrix products, arithmetic and copies ran while one was open for 6% -> 0% of each run, Pallas kernels for 52% -> 0%
where the time goes in v1:
time: 445 us; the launch traced here: 438 us
  Pallas kernels  410 us (92%)
  other arithmetic  13.9 us (3%)
  local copies, waits for them, and re-layouts  13.3 us (3%)
    pallas_call x1, Pallas kernels, serve(): pl.pallas_call(functools.partial(serve_kernel, (gr, fs, tp, local_experts...  298 us
    pallas_call x1, Pallas kernels, combine(): pl.pallas_call(functools.partial(combine_kernel, (fs, tp)), out_shape=jax...  112 us
    unnamed x16, local copies, waits for them, and re-layouts  11.2 us
    transpose x2, other arithmetic, serve(): parts = [w.transpose(0, 2, 1) for w in weights]  11 us

profile of v1, /device:TPU:0, one launch (start us, length us, event | category | flops | bytes accessed | tf_op | source)
XLA Modules:
  0.0 438.1 jit_solution(177840672282506195)
XLA Ops:
  0.6 0.0 copy-start.3
  0.6 1.3 pad.9.refs_2_
  1.9 0.7 fusion.2
  2.6 1.1 reduce-window.6
  3.8 0.2 slice_reduce_fusion
  4.0 0.1 multiply_reduce_fusion.1
  4.1 0.8 add_add_fusion
  5.0 0.6 pad.8.refs_1_
  5.6 4.7 %convert_bitcast_fusion.refs_5_ = bf16[8,704,256]{2,1,0:T(8,128)(2,1)} fusion(f32[8,256,704]{1,2,0:T(8,128)} %param.13), kind=kLoop, calls=%fused_computation.4 | loop fusion | flops 1441792 | bytes 8650752 | tf_op jit(solution)/shard_map/transpose | solution.py:662
  10.3 0.0 copy-done.3
  10.3 0.0 copy-done
  10.3 6.3 %fusion.1 = (bf16[8,704,256]{2,1,0:T(8,128)(2,1)}, bf16[8,704,256]{2,1,0:T(8,128)(2,1)}) fusion(f32[8,256,704]{1,2,0:T(8,128)S(1)} %copy-done, f32[256]{0:T(256)S(1)} %copy-done.3, f32[8,256,704]{1,2,0:T(8,128)} %param.11), kind=kLoop, calls=%fused_computation.3 | loop fusion | flops 5767168 | bytes 17302528 | tf_op jit(solution)/shard_map/transpose | solution.py:662
  16.6 297.9 %serve.1 = (bf16[2,704,2048]{2,1,0:T(8,128)(2,1)}, bf16[2,704,2048]{2,1,0:T(8,128)(2,1)}, bf16[2,704,2048]{2,1,0:T(8,128)(2,1)}, bf16[2,4,704,256]{3,2,1,0:T(8,1...) custom-call(bf16[512,512]{1,0:T(8,128)(2,1)} %refs_0_.1, ...), custom_call_target="tpu_custom_call" | custom-call | tf_op jit(solution)/shard_map/serve/pallas_call | solution.py:671
  314.6 0.0 copy-start.2
  314.6 112.4 %combine.1 = bf16[512,512]{1,0:T(8,128)(2,1)S(1)} custom-call(bf16[4,512,2048]{2,1,0:T(8,128)(2,1)} %get-tuple-element.8.refs_0_), custom_call_target="tpu_custom_call" | custom-call | tf_op jit(solution)/shard_map/combine/pallas_call | solution.py:799
  427.0 0.0 slice-start
  427.0 0.8 copy.17
  427.8 0.0 copy-done.2
  427.8 2.9 copy.18
  430.7 2.4 copy-done.1
  433.1 2.5 copy.19
  435.6 0.0 slice-done
  435.6 0.0 slice-done.1
  435.6 2.5 copy.20
  (7 shorter events, 0.0 us)
Async XLA Ops:
  0.6 9.7 %copy-start.3 = (f32[256]{0:T(256)S(1)}, f32[256]{0:T(256)}, u32[]{:S(2)}) copy-start(f32[256]{0:T(256)} %param.10) | copy-start | bytes 3076
  4.0 6.3 %copy-start = (f32[8,256,704]{1,2,0:T(8,128)S(1)}, f32[8,256,704]{1,2,0:T(8,128)}, u32[]{:S(2)}) copy-start(f32[8,256,704]{1,2,0:T(8,128)} %param.12) | copy-start | bytes 17301508
  314.6 113.2 %copy-start.2 = (bf16[2,704,2048]{2,1,0:T(8,128)(2,1)S(1)}, bf16[2,704,2048]{2,1,0:T(8,128)(2,1)}, u32[]{:S(2)}) copy-start(bf16[2,704,2048]{2,1,0:T(8,128)(2,1)} %get-tuple-element.9) | copy-start | bytes 17301508
  427.0 8.6 %slice-start = ((s8[5767168]{0:T(1024)(128)(4,1)}), s8[4194304]{0:T(1024)(128)(4,1)S(1)}, s32[]{:S(2)}) async-start(s8[5767168]{0:T(1024)(128)(4,1)} %bitcast.44), calls=%async_computation | async-start | bytes 8388608
  427.8 5.3 %copy-start.1 = (bf16[2,704,2048]{2,1,0:T(8,128)(2,1)S(1)}, bf16[2,704,2048]{2,1,0:T(8,128)(2,1)}, u32[]{:S(2)}) copy-start(bf16[2,704,2048]{2,1,0:T(8,128)(2,1)} %get-tuple-element.10) | copy-start | bytes 17301508
  427.8 7.8 %slice-start.1 = ((s8[5767168]{0:T(1024)(128)(4,1)}), s8[1572864]{0:T(1024)(128)(4,1)S(1)}, s32[]{:S(2)}) async-start(s8[5767168]{0:T(1024)(128)(4,1)} %bitcast.44), calls=%async_computation.1 | async-start | bytes 3145728

commit v2 on v0

--- a/solution.py
+++ b/solution.py
@@ -241,7 +241,7 @@
     return [w.swapaxes(1, 2) if flipped else w for w in found[:count]]
 
 
-def local(tokens, routes, route_weight, norm_gain, gate_master, up_master, down_master):
+def local_by_collectives(tokens, routes, route_weight, norm_gain, gate_master, up_master, down_master):
     experts = gate_master.shape[0]
     tp_count = lax.axis_size("tp")
     fs_count = lax.axis_size("fs")
@@ -293,6 +293,681 @@
     return (mixed_out.astype(jnp.bfloat16), gate_w, up_w, down_w)
 
 
+def slot_places(routes, experts, capacity):
+    rows = routes.shape[0]
+    hits = (routes[:, :, None] == jnp.arange(experts, dtype=jnp.int32)).astype(jnp.int32)
+    both = hits[:, 0] + hits[:, 1]
+    before = jnp.cumsum(both, axis=0) - both
+    first = jnp.sum(hits[:, 0] * before, axis=1)
+    second = jnp.sum(hits[:, 1] * (before + hits[:, 0]), axis=1)
+    places = jnp.stack([first, second]) + routes.T * capacity
+    return jnp.pad(places, ((0, 6), (0, 0)))
+
+
+def serve_kernel(sizes, *refs):
+    gr, fs, tp, local_experts, rows, capacity = sizes
+    tokens, places, shares = refs[:3]
+    ins, outs, relays, mixed = refs[3:6], refs[6:9], refs[9:12], refs[12]
+    (
+        bounce_in, bounce_down, gathered, place_of, share_of, picks, slot_share, slots, hid, spread_hid,
+        gate_buf, up_buf, down_buf, part, from_core, to_side, from_side, to_fs, from_near,
+        from_far, kept, kept_far, mixed_buf,
+        tp_send, tp_recv, fs_send, fs_recv, gr_send, gr_recv, load_sem, store_sem,
+        up_sem, low_sem, slab_recv, core_send, side_send, block_recv, info_send, info_recv,
+        own_sem, weight_sem, down_sem, core_psend, core_precv, side_psend, side_precv,
+        near_send, near_recv, far_send, far_recv, mixed_sem,
+    ) = refs[13:]
+    g, f, t = lax.axis_index("gr"), lax.axis_index("fs"), lax.axis_index("tp")
+    bounce = (bounce_in, bounce_down)
+    halves = 2
+    half = rows // halves
+    blocks = [(w, j) for j in range(local_experts) for w in range(2)]
+    blocks += [(2, h) for h in range(halves)]
+    total = len(blocks)
+    token_rows, features = tokens.shape
+    width = fs * features
+
+    barrier = pltpu.get_barrier_semaphore()
+    for axis, me, size in (("gr", g, gr), ("fs", f, fs), ("tp", t, tp)):
+        for d in range(1, size):
+            pl.semaphore_signal(
+                barrier, inc=1, device_id={axis: lax.rem(me + d, size)}, device_id_type=MESH
+            )
+    pl.semaphore_wait(barrier, gr + fs + tp - 3)
+
+    def remote(src, dst, send, recv, axis, target):
+        return pltpu.make_async_remote_copy(
+            src_ref=src, dst_ref=dst, send_sem=send, recv_sem=recv,
+            device_id={axis: target}, device_id_type=MESH,
+        )
+
+    def slab(block, source):
+        return gathered.at[block, source]
+
+    core = t + 1 - 2 * lax.rem(t, 2)
+    side = lax.rem(t + 2, tp)
+    core_side = lax.rem(core + 2, tp)
+
+    def slab_copy(source, up):
+        mine = slab(t, source)
+        sem = (up_sem if up else low_sem).at[source]
+        return remote(mine, mine, sem, slab_recv.at[source], "fs", f + 1 if up else f - 1)
+
+    def slab_pass(source, up):
+        @pl.when(f < fs - 1 if up else f > 0)
+        def _():
+            slab_copy(source, up).start()
+
+    def to_core(k, source):
+        mine = slab((t, side)[k], source)
+        return remote(
+            mine, mine, core_send.at[k, source], block_recv.at[(t, side)[k], source], "tp", core
+        )
+
+    def to_sides(source):
+        mine = slab(t, source)
+        return remote(
+            mine, mine, side_send.at[source], block_recv.at[t, source], "tp", side
+        )
+
+    def slab_spread(source):
+        to_sides(source).start()
+        to_core(0, source).start()
+
+    def slab_arrived(k):
+        for up in (True, False):
+            source = f - k if up else f + k
+
+            @pl.when(source >= 0 if up else source < fs)
+            def _():
+                slab_copy(source, up).wait_recv()
+                slab_pass(source, up)
+                slab_spread(source)
+
+    def block_wait(block, source):
+        mine = slab(block, source)
+        remote(
+            mine, mine, side_send.at[source], block_recv.at[block, source], "tp", side
+        ).wait_recv()
+
+    def side_arrived(k):
+        source = lax.rem(f + k, fs)
+        block_wait(side, source)
+        to_core(1, source).start()
+
+    def core_arrived():
+        for block in (core, core_side):
+            for source in range(fs):
+                block_wait(block, source)
+        for d in range(1, tp):
+            source = lax.rem(t + d, tp)
+            for k in range(2):
+                whole = (place_of, share_of)[k]
+                remote(
+                    (places, shares)[k], whole.at[source], info_send.at[d, k],
+                    info_recv.at[source, k], "tp", source,
+                ).wait_recv()
+
+    def info(d, k):
+        whole = (place_of, share_of)[k]
+        return remote(
+            (places, shares)[k], whole.at[t], info_send.at[d, k], info_recv.at[t, k],
+            "tp", lax.rem(t + d, tp),
+        )
+
+    def own_copies():
+        return (
+            pltpu.make_async_copy(tokens, slab(t, f), own_sem.at[0]),
+            pltpu.make_async_copy(places, place_of.at[t], own_sem.at[1]),
+            pltpu.make_async_copy(shares, share_of.at[t], own_sem.at[2]),
+        )
+
+    def out_rows(c, group, source):
+        w, j = blocks[c]
+        start = pl.multiple_of((group * fs + source) * rows, rows)
+        if w == 2:
+            return outs[w].at[:, :, pl.ds(start + j * half, half)]
+        return outs[w].at[j, :, pl.ds(start, rows)]
+
+    def own(c, target):
+        w, j = blocks[c]
+        if w == 2:
+            first = target * local_experts
+            return ins[w].at[pl.ds(first, local_experts), :, j * half : (j + 1) * half]
+        return ins[w].at[target * local_experts + j]
+
+    def relay(c, source):
+        w, j = blocks[c]
+        if w == 2:
+            return relays[w].at[source, :, :, j * half : (j + 1) * half]
+        return relays[w].at[j, source]
+
+    def tp_copy(c, d, to_out):
+        target = lax.rem(t + d, tp)
+        return remote(
+            own(c, target), out_rows(c, g, f) if to_out else relay(c, t),
+            tp_send.at[c, d], tp_recv.at[c, d], "tp", target,
+        )
+
+    def fs_copy(c, d, src, target):
+        return remote(src, out_rows(c, g, f), fs_send.at[c, d], fs_recv.at[c, f], "fs", target)
+
+    def gr_copy(c, n, source, src):
+        return remote(
+            src, out_rows(c, g, source), gr_send.at[c, n, source], gr_recv.at[c, n, source],
+            "gr", lax.rem(g + n, gr),
+        )
+
+    def to_groups(c, source, src):
+        for n in range(1, gr):
+            gr_copy(c, n, source, src).start()
+
+    def tp_start(c):
+        for d in range(1, tp):
+
+            @pl.when(t == f)
+            def _():
+                tp_copy(c, d, True).start()
+
+            @pl.when(t != f)
+            def _():
+                tp_copy(c, d, False).start()
+
+    def bounce_of(c):
+        w, j = blocks[c]
+        return bounce[1].at[j] if w == 2 else bounce[0].at[c]
+
+    def own_store(c):
+        @pl.when(t == f)
+        def _():
+            pltpu.make_async_copy(own(c, t), bounce_of(c), load_sem.at[c]).wait()
+            pltpu.make_async_copy(bounce_of(c), out_rows(c, g, f), store_sem.at[c]).start()
+
+    def fs_send_next(c, k):
+        odd = lax.rem(f, 2)
+        source = lax.rem(f + (2, 3 - 2 * odd, 1 + 2 * odd)[k], fs)
+        d = lax.rem(t - source + tp, tp)
+
+        @pl.when(source == t)
+        def _():
+            fs_copy(c, d, own(c, t), source).start()
+
+        @pl.when(source != t)
+        def _():
+            remote(
+                own(c, t), relay(c, source), tp_send.at[c, d], tp_recv.at[c, d], "tp", source
+            ).wait_recv()
+            fs_copy(c, d, relay(c, source), source).start()
+
+    def home(c):
+        d = lax.rem(t - f + tp, tp)
+
+        @pl.when(t == f)
+        def _():
+            pltpu.make_async_copy(own(c, t), bounce_of(c), load_sem.at[c]).start()
+            to_groups(c, f, own(c, t))
+
+        @pl.when(t != f)
+        def _():
+            tp_copy(c, d, True).wait_recv()
+            to_groups(c, f, out_rows(c, g, f))
+
+    def fs_arrived(c, k):
+        odd = lax.rem(f, 2)
+        source = lax.rem(f + (2, 3 - 2 * odd, 1 + 2 * odd)[k], fs)
+        remote(
+            own(c, t), out_rows(c, g, source), fs_send.at[c, 0], fs_recv.at[c, source],
+            "fs", source,
+        ).wait_recv()
+        to_groups(c, source, out_rows(c, g, source))
+
+    def gr_arrived(c):
+        for n in range(1, gr):
+            for source in range(fs):
+                group = lax.rem(g + gr - n, gr)
+                remote(
+                    own(c, t), out_rows(c, group, source), gr_send.at[c, n, source],
+                    gr_recv.at[c, n, source], "gr", group,
+                ).wait_recv()
+
+    def own_stored(c):
+        @pl.when(t == f)
+        def _():
+            pltpu.make_async_copy(bounce_of(c), out_rows(c, g, f), store_sem.at[c]).wait()
+
+    def sent(c):
+        for n in range(1, gr):
+            for source in range(fs):
+                gr_copy(c, n, source, out_rows(c, g, source)).wait_send()
+        for d in range(1, tp):
+            tp_copy(c, d, False).wait_send()
+        for d in range(tp):
+            target = lax.rem(t + tp - d, tp)
+
+            @pl.when(target != f)
+            def _():
+                fs_copy(c, d, own(c, t), target).wait_send()
+
+    def pick_slots(j):
+        @pl.loop(0, tp)
+        def _(b):
+            base = (t * local_experts + j) * capacity
+            index = lax.broadcasted_iota(jnp.int32, (capacity, token_rows), 0) + base
+            first = place_of[b, 0:1, :] == index
+            second = place_of[b, 1:2, :] == index
+            share = jnp.where(first, share_of[b, 0:1, :], 0.0)
+            share = share + jnp.where(second, share_of[b, 1:2, :], 0.0)
+            share = jnp.sum(share, axis=1, keepdims=True)
+            at = pl.ds(pl.multiple_of(b * capacity, capacity), capacity)
+            slot_share[at, :] = jnp.broadcast_to(share, (capacity, 128))
+            pick = jnp.where(first | second, 1.0, 0.0).astype(jnp.bfloat16)
+            picks[b] = pick
+            squares = jnp.zeros((capacity, 1), jnp.float32)
+            for q in range(fs):
+                columns = slice(q * features, (q + 1) * features)
+                raw = jnp.dot(
+                    pick, gathered[b, q], preferred_element_type=jnp.float32
+                )
+                slots[at, columns] = raw.astype(jnp.bfloat16)
+                squares = squares + jnp.sum(raw * raw, axis=1, keepdims=True)
+            scale = lax.rsqrt(squares / width + norm_eps)
+            for q in range(fs):
+                columns = slice(q * features, (q + 1) * features)
+                raw = slots[at, columns].astype(jnp.float32)
+                slots[at, columns] = (raw * scale).astype(jnp.bfloat16)
+
+    def weight_load(w, j):
+        return pltpu.make_async_copy(outs[w].at[j], (gate_buf, up_buf)[w], weight_sem.at[w])
+
+    def hidden_of(j, start):
+        units = gate_buf.shape[0]
+        step = 2 * capacity
+        cut = slice(start, min(start + 256, units))
+
+        @pl.loop(0, tp * capacity // step)
+        def _(m):
+            at = pl.ds(pl.multiple_of(m * step, step), step)
+            into = (((1,), (1,)), ((), ()))
+            gate = lax.dot_general(
+                slots[at, :], gate_buf[cut, :], into, preferred_element_type=jnp.float32
+            )
+            up = lax.dot_general(
+                slots[at, :], up_buf[cut, :], into, preferred_element_type=jnp.float32
+            )
+            value = gate / (1.0 + jnp.exp(-gate)) * up
+            hid[at, cut] = (value * slot_share[at, 0:1]).astype(jnp.bfloat16)
+
+    def hidden_to_tokens(j):
+        @pl.loop(0, tp)
+        def _(b):
+            at = pl.ds(pl.multiple_of(b * capacity, capacity), capacity)
+            spread_hid[j, b] = lax.dot_general(
+                picks[b], hid[at, :], (((0,), (0,)), ((), ())),
+                preferred_element_type=jnp.float32,
+            ).astype(jnp.bfloat16)
+
+    pieces = [(h, n) for h in range(halves) for n in range(fs)]
+    upper = f // 2
+    near = f + 1 - 2 * lax.rem(f, 2)
+    inner = (f == 1) | (f == 2)
+
+    def column_owner(n):
+        return (3 - 3 * upper, 2 - upper, near, f)[n]
+
+    joined = features // rows
+    cut = joined * half
+
+    def down_loads(p):
+        h, n = pieces[p]
+        q = column_owner(n)
+        copies = []
+        for i in range(joined):
+            start = pl.multiple_of((q * joined + i) * rows, rows)
+            copies.append(
+                pltpu.make_async_copy(
+                    outs[2].at[:, :, pl.ds(start + h * half, half)],
+                    down_buf.at[p % 2, :, :, i * half : (i + 1) * half],
+                    down_sem.at[p % 2, i],
+                )
+            )
+        return copies
+
+    def core_part(p, k):
+        block = (core, core_side)[k]
+        return remote(
+            part.at[p, block], from_core.at[p, k], core_psend.at[p, k], core_precv.at[p, k],
+            "tp", core,
+        )
+
+    def side_part(p):
+        return remote(
+            to_side.at[p], from_side.at[p], side_psend.at[p], side_precv.at[p], "tp", side
+        )
+
+    def near_part(p):
+        return remote(to_fs.at[p], from_near.at[p], near_send.at[p], near_recv.at[p], "fs", near)
+
+    def far_part(p):
+        h, n = pieces[p]
+        return remote(
+            to_fs.at[p], from_far.at[h], far_send.at[p], far_recv.at[h], "fs", column_owner(n)
+        )
+
+    def piece_start(p):
+        for copy in down_loads(p):
+            copy.wait()
+        if p + 1 < len(pieces) and pieces[p + 1][0] == pieces[p][0]:
+            for copy in down_loads(p + 1):
+                copy.start()
+
+        @pl.loop(0, tp)
+        def _(b):
+            value = jnp.dot(
+                spread_hid[0, b], down_buf[p % 2, 0], preferred_element_type=jnp.float32
+            )
+            for j in range(1, local_experts):
+                value = value + jnp.dot(
+                    spread_hid[j, b], down_buf[p % 2, j], preferred_element_type=jnp.float32
+                )
+            part[p, b] = value.astype(jnp.bfloat16)
+
+        for k in range(2):
+            core_part(p, k).start()
+
+    def piece_side(p):
+        for k in range(2):
+            core_part(p, k).wait_recv()
+        value = part[p, side].astype(jnp.float32) + from_core[p, 1].astype(jnp.float32)
+        to_side[p] = value.astype(jnp.bfloat16)
+        side_part(p).start()
+
+    def piece_fs(p):
+        h, n = pieces[p]
+        side_part(p).wait_recv()
+        value = part[p, t].astype(jnp.float32) + from_core[p, 0].astype(jnp.float32)
+        value = value + from_side[p].astype(jnp.float32)
+        if n == 3:
+            kept[h] = value
+        elif n == 2:
+            to_fs[p] = value.astype(jnp.bfloat16)
+            near_part(p).start()
+        else:
+            @pl.when(inner)
+            def _():
+                kept_far[p % 2] = value
+
+            @pl.when(jnp.logical_not(inner))
+            def _():
+                to_fs[p] = value.astype(jnp.bfloat16)
+                near_part(p).start()
+
+    def piece_far(p):
+        h, n = pieces[p]
+
+        @pl.when(inner)
+        def _():
+            near_part(p).wait_recv()
+            value = kept_far[p % 2] + from_near[p].astype(jnp.float32)
+            to_fs[p] = value.astype(jnp.bfloat16)
+            far_part(p).start()
+
+    def finish(h):
+        value = kept[h]
+        near_part(h * fs + 2).wait_recv()
+        value = value + from_near[h * fs + 2].astype(jnp.float32)
+        far_part(h * fs).wait_recv()
+        value = value + from_far[h].astype(jnp.float32)
+        value = value.astype(jnp.bfloat16)
+        for i in range(joined):
+            first = i * rows + h * half
+            mixed_buf[:, first : first + half] = value[:, i * half : (i + 1) * half]
+
+    def all_pieces(h):
+        own_pieces = [p for p in range(len(pieces)) if pieces[p][0] == h]
+        thunks = [lambda: [copy.start() for copy in down_loads(own_pieces[0])]]
+        for n in range(len(own_pieces) + 2):
+            if n < len(own_pieces):
+                thunks.append(functools.partial(piece_start, own_pieces[n]))
+            if 1 <= n <= len(own_pieces):
+                thunks.append(functools.partial(piece_side, own_pieces[n - 1]))
+            if n >= 2:
+                thunks.append(functools.partial(piece_fs, own_pieces[n - 2]))
+            if n in (3, 4):
+                thunks.append(functools.partial(piece_far, own_pieces[n - 3]))
+        return thunks
+
+    def expert_thunks(j):
+        def begin():
+            for w in range(2):
+                gr_arrived(2 * j + w)
+                own_stored(2 * j + w)
+                weight_load(w, j).start()
+            pick_slots(j)
+            weight_load(0, j).wait()
+            weight_load(1, j).wait()
+
+        units = gate_buf.shape[0]
+        cuts = [functools.partial(hidden_of, j, start) for start in range(0, units, 256)]
+        return [begin, *cuts, functools.partial(hidden_to_tokens, j)]
+
+    own_load = own_copies()
+    for copy in own_load:
+        copy.start()
+    for up in (True, False):
+        @pl.when(f < fs - 1 if up else f > 0)
+        def _():
+            remote(
+                tokens, slab(t, f), (up_sem if up else low_sem).at[f], slab_recv.at[f],
+                "fs", f + 1 if up else f - 1,
+            ).start()
+    for d in range(1, tp):
+        for k in range(2):
+            info(d, k).start()
+    early = min(4, total)
+    for c in range(early):
+        tp_start(c)
+    own_load[0].wait()
+    slab_spread(f)
+
+    def out_waits(c):
+        return [
+            functools.partial(home, c),
+            *[functools.partial(fs_send_next, c, k) for k in range(fs - 1)],
+        ]
+
+    def fs_waits(c):
+        return [functools.partial(fs_arrived, c, k) for k in range(fs - 1)]
+
+    def mix(waits, todo):
+        for n, wait in enumerate(waits):
+            wait()
+            take = -(-len(todo) // (len(waits) - n))
+            for thunk in todo[:take]:
+                thunk()
+            todo = todo[take:]
+        for thunk in todo:
+            thunk()
+
+    def both(first, second):
+        longer = max(len(first), len(second))
+        found = []
+        for n in range(longer):
+            found += first[n : n + 1] + second[n : n + 1]
+        return found
+
+    mix(out_waits(0), [])
+    slab_arrived(1)
+    mix(out_waits(1), [])
+    slab_arrived(2)
+    own_store(0)
+    mix(both(fs_waits(0), out_waits(2)), [])
+    slab_arrived(3)
+    for c in range(early, total):
+        tp_start(c)
+    own_store(1)
+    own_store(2)
+    mix(both(fs_waits(1), out_waits(3)), [])
+    own_load[1].wait()
+    own_load[2].wait()
+    for k in range(fs):
+        side_arrived(k)
+    own_store(3)
+    mix(both(fs_waits(2), out_waits(4)), [])
+    own_store(4)
+    core_arrived()
+    mix(both(fs_waits(3), out_waits(5)), expert_thunks(0))
+    own_store(5)
+    mix(fs_waits(4), expert_thunks(1))
+    gr_arrived(4)
+    own_stored(4)
+    mix(fs_waits(5), all_pieces(0))
+    for h in range(1, halves):
+        c = 2 * local_experts + h
+        gr_arrived(c)
+        own_stored(c)
+        for thunk in all_pieces(h):
+            thunk()
+    for h in range(halves):
+        finish(h)
+    store = pltpu.make_async_copy(mixed_buf, mixed, mixed_sem)
+    store.start()
+
+    for c in range(total):
+        sent(c)
+    for source in range(fs):
+        for up in (True, False):
+            @pl.when((f < fs - 1) & (source <= f) if up else (f > 0) & (source >= f))
+            def _():
+                slab_copy(source, up).wait_send()
+        to_sides(source).wait_send()
+        to_core(0, source).wait_send()
+        to_core(1, source).wait_send()
+    for d in range(1, tp):
+        for k in range(2):
+            info(d, k).wait_send()
+    for p in range(len(pieces)):
+        for k in range(2):
+            core_part(p, k).wait_send()
+        side_part(p).wait_send()
+        if pieces[p][1] == 2:
+            near_part(p).wait_send()
+        elif pieces[p][1] < 2:
+            @pl.when(inner)
+            def _():
+                far_part(p).wait_send()
+
+            @pl.when(jnp.logical_not(inner))
+            def _():
+                near_part(p).wait_send()
+    store.wait()
+
+
+def serve(tokens, places, shares, capacity, *weights):
+    gr, fs, tp = lax.axis_size("gr"), lax.axis_size("fs"), lax.axis_size("tp")
+    experts, rows, columns = weights[0].shape
+    local_experts = experts // tp
+    token_rows, features = tokens.shape
+    width = features * fs
+    parts = [w.transpose(0, 2, 1) for w in weights]
+    block = (columns, rows)
+    bf16, f32 = jnp.bfloat16, jnp.float32
+    served = jax.ShapeDtypeStruct((local_experts, columns, width), bf16)
+    relayed = jax.ShapeDtypeStruct((local_experts, tp, *block), bf16)
+    relayed_down = jax.ShapeDtypeStruct((tp, local_experts, *block), bf16)
+    half, pieces = rows // 2, 2 * fs
+    cut = features // rows * half
+    total = 2 * local_experts + 2
+    dma = pltpu.SemaphoreType.DMA
+    anywhere = pl.BlockSpec(memory_space=pl.ANY)
+    slots = tp * capacity
+    found = pl.pallas_call(
+        functools.partial(serve_kernel, (gr, fs, tp, local_experts, rows, capacity)),
+        out_shape=[served] * 3
+        + [relayed] * 2
+        + [relayed_down, jax.ShapeDtypeStruct((token_rows, features), bf16)],
+        in_specs=[anywhere] * 6,
+        out_specs=[anywhere] * 7,
+        scratch_shapes=[
+            pltpu.VMEM((2 * local_experts, *block), bf16),
+            pltpu.VMEM((2, local_experts, columns, half), bf16),
+            pltpu.VMEM((tp, fs, token_rows, features), bf16),
+            pltpu.VMEM((tp, *places.shape), jnp.int32),
+            pltpu.VMEM((tp, *shares.shape), f32),
+            pltpu.VMEM((tp, capacity, token_rows), bf16),
+            pltpu.VMEM((slots, 128), f32),
+            pltpu.VMEM((slots, width), bf16),
+            pltpu.VMEM((slots, columns), bf16),
+            pltpu.VMEM((local_experts, tp, token_rows, columns), bf16),
+            pltpu.VMEM((columns, width), bf16),
+            pltpu.VMEM((columns, width), bf16),
+            pltpu.VMEM((2, local_experts, columns, cut), bf16),
+            pltpu.VMEM((pieces, tp, token_rows, cut), bf16),
+            pltpu.VMEM((pieces, 2, token_rows, cut), bf16),
+            pltpu.VMEM((pieces, token_rows, cut), bf16),
+            pltpu.VMEM((pieces, token_rows, cut), bf16),
+            pltpu.VMEM((pieces, token_rows, cut), bf16),
+            pltpu.VMEM((pieces, token_rows, cut), bf16),
+            pltpu.VMEM((2, token_rows, cut), bf16),
+            pltpu.VMEM((2, token_rows, cut), f32),
+            pltpu.VMEM((2, token_rows, cut), f32),
+            pltpu.VMEM((token_rows, features), bf16),
+            dma((total, tp)),
+            dma((total, tp)),
+            dma((total, tp)),
+            dma((total, fs)),
+            dma((total, gr, fs)),
+            dma((total, gr, fs)),
+            dma((total,)),
+            dma((total,)),
+            dma((fs,)),
+            dma((fs,)),
+            dma((fs,)),
+            dma((2, fs)),
+            dma((fs,)),
+            dma((tp, fs)),
+            dma((tp, 2)),
+            dma((tp, 2)),
+            dma((3,)),
+            dma((2,)),
+            dma((2, features // rows)),
+            dma((pieces, 2)),
+            dma((pieces, 2)),
+            dma((pieces,)),
+            dma((pieces,)),
+            dma((pieces,)),
+            dma((pieces,)),
+            dma((pieces,)),
+            dma((2,)),
+            dma,
+        ],
+        compiler_params=pltpu.CompilerParams(
+            collective_id=0, has_side_effects=True, vmem_limit_bytes=60 * 1024 * 1024
+        ),
+        name="serve",
+    )(tokens, places, shares, *parts)
+    return [w.swapaxes(1, 2) for w in found[:3]], found[6]
+
+
+def local(tokens, routes, route_weight, norm_gain, gate_master, up_master, down_master):
+    experts, rows, columns = gate_master.shape
+    gr, fs, tp = lax.axis_size("gr"), lax.axis_size("fs"), lax.axis_size("tp")
+    token_rows, features = tokens.shape
+    capacity = 3 * token_rows // experts
+    fits = fs == tp and rows % 128 == 0 and features % 128 == 0 and features % rows == 0
+    if not (fits and tp == 4 and rows % 256 == 0 and capacity % 16 == 0 and columns % 16 == 0):
+        return local_by_collectives(
+            tokens, routes, route_weight, norm_gain, gate_master, up_master, down_master
+        )
+    scaled_gain = norm_gain[None, :, None]
+    gate_w = (gate_master * scaled_gain).astype(jnp.bfloat16)
+    up_w = (up_master * scaled_gain).astype(jnp.bfloat16)
+    down_w = down_master.astype(jnp.bfloat16)
+    places = slot_places(routes, experts, capacity)
+    shares = jnp.pad(route_weight.T, ((0, 6), (0, 0)))
+    served, mixed = serve(tokens, places, shares, capacity, gate_w, up_w, down_w)
+    return (mixed, *served)
+
+
 def solution(mesh):
     placed = (
         P(("gr", "tp"), "fs"),

time: 574 us -> 339 us (0.59)
  waiting for transfers between devices: 140 us -> 0 us
  matrix products: 38.2 us -> 0 us
  blocking collectives: 36.1 us -> 0 us
  between operations: 13.9 us -> 0.67 us
  Pallas kernels: 297 us -> 308 us
  starting transfers between devices: 7.51 us -> 0 us
  other arithmetic: 21.2 us -> 13.9 us
    reduce_scatter x2 -> x0, waiting for transfers between devices: 128 us -> none  [local(): lax.psum_scatter(partial_value.astype(jnp.bfloat16), 'fs', scatter_dimens...]
    dot_general x5 -> x0, matrix products: 38.2 us -> none  [the longest x2 23.5 us: local(): jnp.einsum('scf,df->scd', hidden, down_w[j], preferred_element_type=jnp.f...]
    all_to_all x1 -> x0, blocking collectives: 22.6 us -> none  [local(): lax.all_to_all(outgoing, 'tp', split_axis=0, concat_axis=0, tiled=True)]
    psum x1 -> x0, blocking collectives: 13.5 us -> none  [local(): square_total = lax.psum(jnp.sum(as_float * as_float, axis=1), 'fs')]
    all_to_all x2 -> x0, waiting for transfers between devices: 11.5 us -> none  [local(): lax.all_to_all(summed, 'tp', split_axis=0, concat_axis=0, tiled=True)]
    pallas_call x1, Pallas kernels: 297 us -> 308 us  [serve(): pl.pallas_call(functools.partial(serve_kernel, (gr, fs, tp, local_experts...]
    all_to_all x2 -> x0, starting transfers between devices: 6.99 us -> none  [local(): lax.all_to_all(summed, 'tp', split_axis=0, concat_axis=0, tiled=True)]
    unnamed x18 -> x14, local copies, waits for them, and re-layouts: 12.3 us -> 13.8 us
  transfers between devices with their start and end apart: 5 -> 0, of which waited for: 3 -> 0; matrix products, arithmetic and copies ran while one was open for 6% -> 0% of each run, Pallas kernels for 52% -> 0%
where the time goes in v2:
time: 339 us; the launch traced here: 338 us
  Pallas kernels  308 us (91%)
  local copies, waits for them, and re-layouts  15.9 us (5%)
  other arithmetic  13.9 us (4%)
    pallas_call x1, Pallas kernels, serve(): pl.pallas_call(functools.partial(serve_kernel, (gr, fs, tp, local_experts...  308 us
    unnamed x14, local copies, waits for them, and re-layouts  13.8 us
    transpose x2, other arithmetic, serve(): parts = [w.transpose(0, 2, 1) for w in weights]  11 us

profile of v2, /device:TPU:0, one launch (start us, length us, event | category | flops | bytes accessed | tf_op | source)
XLA Modules:
  0.0 338.4 jit_solution(7273732699614189589)
XLA Ops:
  0.6 0.0 copy-start.2
  0.6 1.3 pad.9.refs_2_
  1.9 0.7 fusion.2
  2.6 1.1 reduce-window.6
  3.8 0.2 slice_reduce_fusion
  4.0 0.0 copy-start
  4.0 0.1 multiply_reduce_fusion.1
  4.1 0.8 add_add_fusion
  5.0 0.6 pad.8.refs_1_
  5.6 4.7 %convert_bitcast_fusion.refs_5_ = bf16[8,704,256]{2,1,0:T(8,128)(2,1)} fusion(f32[8,256,704]{1,2,0:T(8,128)} %param.13), kind=kLoop, calls=%fused_computation.4 | loop fusion | flops 1441792 | bytes 8650752 | tf_op jit(solution)/shard_map/transpose | solution.py:871
  10.3 0.0 copy-done.2
  10.3 0.0 copy-done
  10.3 6.3 %fusion.1 = (bf16[8,704,256]{2,1,0:T(8,128)(2,1)}, bf16[8,704,256]{2,1,0:T(8,128)(2,1)}) fusion(f32[8,256,704]{1,2,0:T(8,128)S(1)} %copy-done, f32[256]{0:T(256)S(1)} %copy-done.2, f32[8,256,704]{1,2,0:T(8,128)} %param.11), kind=kLoop, calls=%fused_computation.3 | loop fusion | flops 5767168 | bytes 17302528 | tf_op jit(solution)/shard_map/transpose | solution.py:871
  16.6 308.0 %serve.1 = (bf16[2,704,2048]{2,1,0:T(8,128)(2,1)}, bf16[2,704,2048]{2,1,0:T(8,128)(2,1)}, bf16[2,704,2048]{2,1,0:T(8,128)(2,1)}, bf16[2,4,704,256]{3,2,1,0:T(8,1...) custom-call(bf16[512,512]{1,0:T(8,128)(2,1)} %refs_0_.1, ...), custom_call_target="tpu_custom_call" | custom-call | tf_op jit(solution)/shard_map/serve/pallas_call | solution.py:883
  324.6 1.9 copy.17
  326.5 0.0 copy-start.1
  326.5 0.0 slice-start
  326.5 6.6 %copy.18 = bf16[2,2048,704]{1,2,0:T(8,128)(2,1)} copy(bf16[2,2048,704]{1,2,0:T(8,128)(2,1)} %bitcast.48) | data formatting | bytes 11534336
  333.1 0.0 copy-done.1
  333.1 0.0 slice-start.1
  333.1 2.5 copy.19
  335.7 0.0 slice-done
  335.7 0.2 slice-done.1
  335.9 2.5 copy.20
  (4 shorter events, 0.0 us)
Async XLA Ops:
  0.6 9.7 %copy-start.2 = (f32[256]{0:T(256)S(1)}, f32[256]{0:T(256)}, u32[]{:S(2)}) copy-start(f32[256]{0:T(256)} %param.10) | copy-start | bytes 3076
  4.0 6.3 %copy-start = (f32[8,256,704]{1,2,0:T(8,128)S(1)}, f32[8,256,704]{1,2,0:T(8,128)}, u32[]{:S(2)}) copy-start(f32[8,256,704]{1,2,0:T(8,128)} %param.12) | copy-start | bytes 17301508
  326.5 6.6 %copy-start.1 = (bf16[2,704,2048]{2,1,0:T(8,128)(2,1)S(1)}, bf16[2,704,2048]{2,1,0:T(8,128)(2,1)}, u32[]{:S(2)}) copy-start(bf16[2,704,2048]{2,1,0:T(8,128)(2,1)} %get-tuple-element.10) | copy-start | bytes 17301508
  326.5 9.2 %slice-start = ((s8[5767168]{0:T(1024)(128)(4,1)}), s8[4194304]{0:T(1024)(128)(4,1)S(1)}, s32[]{:S(2)}) async-start(s8[5767168]{0:T(1024)(128)(4,1)} %bitcast.44), calls=%async_computation | async-start | bytes 8388608
  333.1 2.7 slice-start.1

commit v3 on v2

--- a/solution.py
+++ b/solution.py
@@ -797,30 +797,34 @@
 
     mix(out_waits(0), [])
     slab_arrived(1)
+    own_store(0)
     mix(out_waits(1), [])
+    mix(fs_waits(0), [])
     slab_arrived(2)
-    own_store(0)
-    mix(both(fs_waits(0), out_waits(2)), [])
+    own_store(1)
+    mix(out_waits(2), [])
+    mix(fs_waits(1), [])
     slab_arrived(3)
     for c in range(early, total):
         tp_start(c)
-    own_store(1)
     own_store(2)
-    mix(both(fs_waits(1), out_waits(3)), [])
+    mix(out_waits(3), [])
+    mix(fs_waits(2), [])
     own_load[1].wait()
     own_load[2].wait()
-    for k in range(fs):
-        side_arrived(k)
+    sides = [functools.partial(side_arrived, k) for k in range(fs)]
     own_store(3)
-    mix(both(fs_waits(2), out_waits(4)), [])
+    mix(out_waits(4), sides)
+    mix(fs_waits(3), [])
+    core_arrived()
     own_store(4)
-    core_arrived()
-    mix(both(fs_waits(3), out_waits(5)), expert_thunks(0))
+    mix(out_waits(5), [])
+    mix(fs_waits(4), expert_thunks(0))
     own_store(5)
-    mix(fs_waits(4), expert_thunks(1))
+    mix(fs_waits(5), expert_thunks(1))
     gr_arrived(4)
     own_stored(4)
-    mix(fs_waits(5), all_pieces(0))
+    mix(all_pieces(0), [])
     for h in range(1, halves):
         c = 2 * local_experts + h
         gr_arrived(c)

time: 339 us -> 327 us (0.965)
  Pallas kernels: 308 us -> 297 us
    pallas_call x1, Pallas kernels: 308 us -> 297 us  [serve(): pl.pallas_call(functools.partial(serve_kernel, (gr, fs, tp, local_experts...]
where the time goes in v3:
time: 327 us
  Pallas kernels  297 us (91%)
  local copies, waits for them, and re-layouts  15.9 us (5%)
  other arithmetic  13.9 us (4%)
    pallas_call x1, Pallas kernels, serve(): pl.pallas_call(functools.partial(serve_kernel, (gr, fs, tp, local_experts...  297 us
    unnamed x14, local copies, waits for them, and re-layouts  13.8 us
    transpose x2, other arithmetic, serve(): parts = [w.transpose(0, 2, 1) for w in weights]  11 us

profile of v3, /device:TPU:0, one launch (start us, length us, event | category | flops | bytes accessed | tf_op | source)
XLA Modules:
  0.0 327.1 jit_solution(13423668835818874321)
XLA Ops:
  0.6 0.0 copy-start.2
  0.6 1.3 pad.9.refs_2_
  1.9 0.7 fusion.2
  2.6 1.1 reduce-window.6
  3.8 0.2 slice_reduce_fusion
  4.0 0.0 copy-start
  4.0 0.1 multiply_reduce_fusion.1
  4.1 0.8 add_add_fusion
  5.0 0.6 pad.8.refs_1_
  5.6 4.7 %convert_bitcast_fusion.refs_5_ = bf16[8,704,256]{2,1,0:T(8,128)(2,1)} fusion(f32[8,256,704]{1,2,0:T(8,128)} %param.13), kind=kLoop, calls=%fused_computation.4 | loop fusion | flops 1441792 | bytes 8650752 | tf_op jit(solution)/shard_map/transpose | solution.py:875
  10.3 0.0 copy-done.2
  10.3 0.0 copy-done
  10.3 6.3 %fusion.1 = (bf16[8,704,256]{2,1,0:T(8,128)(2,1)}, bf16[8,704,256]{2,1,0:T(8,128)(2,1)}) fusion(f32[8,256,704]{1,2,0:T(8,128)S(1)} %copy-done, f32[256]{0:T(256)S(1)} %copy-done.2, f32[8,256,704]{1,2,0:T(8,128)} %param.11), kind=kLoop, calls=%fused_computation.3 | loop fusion | flops 5767168 | bytes 17302528 | tf_op jit(solution)/shard_map/transpose | solution.py:875
  16.6 296.7 %serve.1 = (bf16[2,704,2048]{2,1,0:T(8,128)(2,1)}, bf16[2,704,2048]{2,1,0:T(8,128)(2,1)}, bf16[2,704,2048]{2,1,0:T(8,128)(2,1)}, bf16[2,4,704,256]{3,2,1,0:T(8,1...) custom-call(bf16[512,512]{1,0:T(8,128)(2,1)} %refs_0_.1, ...), custom_call_target="tpu_custom_call" | custom-call | tf_op jit(solution)/shard_map/serve/pallas_call | solution.py:887
  313.4 1.9 copy.17
  315.2 0.0 copy-start.1
  315.2 0.0 slice-start
  315.2 6.6 %copy.18 = bf16[2,2048,704]{1,2,0:T(8,128)(2,1)} copy(bf16[2,2048,704]{1,2,0:T(8,128)(2,1)} %bitcast.48) | data formatting | bytes 11534336
  321.9 0.0 copy-done.1
  321.9 0.0 slice-start.1
  321.9 2.5 copy.19
  324.4 0.0 slice-done
  324.4 0.2 slice-done.1
  324.6 2.5 copy.20
  (4 shorter events, 0.0 us)
Async XLA Ops:
  0.6 9.7 %copy-start.2 = (f32[256]{0:T(256)S(1)}, f32[256]{0:T(256)}, u32[]{:S(2)}) copy-start(f32[256]{0:T(256)} %param.10) | copy-start | bytes 3076
  4.0 6.3 %copy-start = (f32[8,256,704]{1,2,0:T(8,128)S(1)}, f32[8,256,704]{1,2,0:T(8,128)}, u32[]{:S(2)}) copy-start(f32[8,256,704]{1,2,0:T(8,128)} %param.12) | copy-start | bytes 17301508
  315.2 6.6 %copy-start.1 = (bf16[2,704,2048]{2,1,0:T(8,128)(2,1)S(1)}, bf16[2,704,2048]{2,1,0:T(8,128)(2,1)}, u32[]{:S(2)}) copy-start(bf16[2,704,2048]{2,1,0:T(8,128)(2,1)} %get-tuple-element.10) | copy-start | bytes 17301508
  315.2 9.2 %slice-start = ((s8[5767168]{0:T(1024)(128)(4,1)}), s8[4194304]{0:T(1024)(128)(4,1)S(1)}, s32[]{:S(2)}) async-start(s8[5767168]{0:T(1024)(128)(4,1)} %bitcast.44), calls=%async_computation | async-start | bytes 8388608
  321.9 2.7 slice-start.1
